TPU v7x, 512 devices: a whole 4x8x8 slice. The times are simulated.
512 devices in a mesh: sp: 64 (over z, y), tp: 8 (over x, core).
Axes of the slice: x: 4, y: 8, z: 8, core: 2. Of those that a mesh axis runs over, the one named last changes fastest.
Arguments:
- resid: bfloat16 [32768, 2048], P(('sp', 'tp')), may hold values from -3 to 3
- queries: bfloat16 [32768, 1024], P('sp', 'tp'), may hold values from -6 to 6
- keys: bfloat16 [32768, 512], P('sp', 'tp'), may hold values from -6 to 6
- values: bfloat16 [32768, 512], P('sp', 'tp'), may hold values from -6 to 6
- documents: int32 [32768], P('sp'), may hold values from 0 to 31, never falling along the last dimension, each value on 1 to 2048 neighbouring positions
- sinks: float32 [16], P('tp'), may hold values from 0 to 5
- out_proj: bfloat16 [1024, 2048], replicated, may hold values from -0.75 to 0.75
- norm_gain: float32 [2048], replicated, may hold values from 0.1 to 1.9
- gate_proj: bfloat16 [2048, 5632], P('sp', 'tp'), may hold values from -0.125 to 0.125
- up_proj: bfloat16 [2048, 5632], P('sp', 'tp'), may hold values from -0.125 to 0.125
- down_proj: bfloat16 [5632, 2048], P('tp', 'sp'), may hold values from -0.078125 to 0.078125
Outputs:
- mixed: bfloat16 [32768, 2048], P(('sp', 'tp'))
Inputs may be any that keep to these rules, and one draw needn't show every extreme that they name: `documents`: document numbers never fall along the sequence; each document holds at most 2048 positions.
All inputs are finite; a program needn't handle non-finite values.
Results may differ from a plain program's by a relative error of at most 0.0095.
Values may be sent and summed in bfloat16 or wider, within the bound.
A program may use at most 64 MiB of HBM per device.

v0:
```python
import jax
import jax.numpy as jnp
from jax import lax
from jax.sharding import PartitionSpec as P

HD = 64
WINDOW = 128


def passed_along(value, axis, steps):
    count = lax.axis_size(axis)
    first, last = (max(0, -steps), min(count, count - steps))
    return lax.ppermute(value, axis, [(source, source + steps) for source in range(first, last)])


def rows_first(arrays, axis, dims):
    turned = [jnp.moveaxis(a, dim, 0) for a, dim in zip(arrays, dims)]
    widths = [t[0].size for t in turned]
    both = jnp.concatenate([t.reshape(-1, w) for t, w in zip(turned, widths)], axis=1)
    whole = lax.all_gather(both, axis, axis=0, tiled=True)
    tiles = jnp.split(whole, [sum(widths[:k]) for k in range(1, len(widths))], axis=1)
    return tuple(
        (
            jnp.moveaxis(b.reshape(-1, *t.shape[1:]), 0, dim)
            for b, t, dim in zip(tiles, turned, dims)
        )
    )


def in_order(tiles, dim):
    dims = list(tiles.shape[1:])
    dims[dim] *= tiles.shape[0]
    return jnp.moveaxis(tiles, 0, dim).reshape(dims)


def from_everyone(x, axis):
    size = lax.axis_size(axis)
    return lax.all_to_all(jnp.broadcast_to(x[None], (size, *x.shape)), axis, 0, 0, tiled=True)


def gather_directly(x, axis, dim):
    return in_order(from_everyone(x, axis), dim)


def in_blocks(x, dim, size):
    before, after = (x.shape[:dim], x.shape[dim + 1 :])
    return jnp.moveaxis(x.reshape(*before, size, -1, *after), dim, 0)


def sum_at_owner(x, axis, dim):
    size = lax.axis_size(axis)
    tiles = lax.all_to_all(in_blocks(x, dim, size), axis, 0, 0, tiled=True)
    return jnp.sum(tiles.astype(jnp.float32), axis=0)


def attend(queries, keys, values, documents, sinks):
    rows = queries.shape[0]
    kv_heads = keys.shape[1] // HD
    group = queries.shape[1] // HD // kv_heads
    blocks = rows // WINDOW
    key_value = jnp.concatenate([keys, values], axis=1)
    tail_pair, tail_docs = passed_along(
        (key_value[rows - WINDOW :], documents[rows - WINDOW :].astype(jnp.bfloat16)), "sp", 1
    )
    ext_pair = jnp.concatenate([tail_pair, key_value], axis=0).reshape(
        blocks + 1, WINDOW, 2 * kv_heads * HD
    )
    ext_docs = jnp.concatenate([tail_docs.astype(jnp.int32), documents], axis=0).reshape(
        blocks + 1, WINDOW
    )
    band = jnp.concatenate([ext_pair[:-1], ext_pair[1:]], axis=1)
    band_keys = band[:, :, : kv_heads * HD].reshape(blocks, 2 * WINDOW, kv_heads, HD)
    band_values = band[:, :, kv_heads * HD :].reshape(blocks, 2 * WINDOW, kv_heads, HD)
    band_docs = jnp.concatenate([ext_docs[:-1], ext_docs[1:]], axis=1)
    query_docs = documents.reshape(blocks, WINDOW)
    offset = lax.axis_index("sp") * rows
    distance = jnp.arange(WINDOW)[:, None] + WINDOW - jnp.arange(2 * WINDOW)[None, :]
    key_pos = (
        offset + jnp.arange(blocks)[:, None] * WINDOW + jnp.arange(2 * WINDOW)[None, :] - WINDOW
    )
    visible = (
        ((distance >= 0) & (distance < WINDOW))[None]
        & (key_pos >= 0)[:, None, :]
        & (band_docs[:, None, :] == query_docs[:, :, None])
    )
    query_blocks = queries.reshape(blocks, WINDOW, kv_heads, group, HD)
    scores = jnp.einsum(
        "nikgd,njkd->nkgij", query_blocks, band_keys, preferred_element_type=jnp.float32
    ) * HD ** (-0.5)
    scores = jnp.where(visible[:, None, None], scores, -jnp.inf)
    sink_logit = sinks.reshape(kv_heads, group)[None, :, :, None, None]
    row_top = jnp.maximum(jnp.max(scores, axis=-1, keepdims=True), sink_logit)
    raw_weights = jnp.exp(scores - row_top)
    totals = jnp.sum(raw_weights, axis=-1, keepdims=True) + jnp.exp(sink_logit - row_top)
    weights = (raw_weights / totals).astype(jnp.bfloat16)
    attended = jnp.einsum(
        "nkgij,njkd->nikgd", weights, band_values, preferred_element_type=jnp.float32
    )
    return attended.astype(jnp.bfloat16).reshape(rows, kv_heads * group * HD)


def norm_rows(mid_rows, norm_gain):
    scale = lax.rsqrt(jnp.mean(mid_rows * mid_rows, axis=-1, keepdims=True) + 1e-06)
    return (mid_rows * scale * norm_gain).astype(jnp.bfloat16)


def shards(
    resid,
    queries,
    keys,
    values,
    documents,
    sinks,
    out_proj,
    norm_gain,
    gate_proj,
    up_proj,
    down_proj,
):
    gate_whole, up_whole, down_whole = rows_first((gate_proj, up_proj, down_proj), "sp", (0, 0, 1))
    attended = attend(queries, keys, values, documents, sinks)
    own_heads = lax.all_to_all(attended, "tp", split_axis=0, concat_axis=1, tiled=True)
    mid_rows = resid.astype(jnp.float32) + jnp.dot(
        own_heads, out_proj, preferred_element_type=jnp.float32
    )
    normed = gather_directly(norm_rows(mid_rows, norm_gain), "tp", 0)
    gate_acts = jnp.dot(normed, gate_whole, preferred_element_type=jnp.float32)
    up_acts = jnp.dot(normed, up_whole, preferred_element_type=jnp.float32)
    hidden = (jax.nn.silu(gate_acts) * up_acts).astype(jnp.bfloat16)
    summed = sum_at_owner(
        jnp.dot(hidden, down_whole, preferred_element_type=jnp.float32).astype(jnp.bfloat16),
        "tp",
        0,
    )
    return (mid_rows + summed).astype(jnp.bfloat16)


def solution(mesh):
    in_specs = (
        P(("sp", "tp"), None),
        P("sp", "tp"),
        P("sp", "tp"),
        P("sp", "tp"),
        P("sp"),
        P("tp"),
        P(),
        P(),
        P("sp", "tp"),
        P("sp", "tp"),
        P("tp", "sp"),
    )
    out_specs = P(("sp", "tp"), None)
    return jax.shard_map(shards, mesh=mesh, in_specs=in_specs, out_specs=out_specs, check_vma=False)
```

profile of v0, /device:TPU:1, one launch (start us, length us, event | category | flops | bytes accessed | tf_op | source)
XLA Modules:
  0.0 170.7 jit_solution(16067916554664489220)
XLA Ops:
  6.5 1.6 concatenate.23
  8.2 0.7 convert.3
  8.9 4.0 %collective-permute-start.1 = (bf16[128]{0:T(256)(128)(2,1)S(1)}, bf16[128]{0:T(256)(128)(2,1)S(1)}, u32[]{:S(2)}, u32[]{:S(2)}) collective-permute-start(bf16[128]{0:T(256)(128)(2,1)S(1)} %slice.48), channel_id=1, source_target_pairs={{0,8},{8,16},{16,24},{24,32},{32,40},{40,48},{48,56},{56,64},{64,7... | collective-permute-start | bytes 776 | tf_op jit(solution)/shard_map/ppermute | solution.py:13
  12.9 1.0 copy.23
  13.9 1.0 copy.24
  14.9 3.2 %collective-permute-start = (bf16[128,128]{1,0:T(8,128)(2,1)S(1)}, bf16[128,128]{1,0:T(8,128)(2,1)S(1)}, u32[]{:S(2)}, u32[]{:S(2)}) collective-permute-start(bf16[128,128]{1,0:T(8,128)(2,1)S(1)} %fusion.35), channel_id=1, source_target_pairs={{0,8},{8,16},{16,24},{24,32},{32,40},{40,48},{48,56},{56,64},{64,7... | collective-permute-start | bytes 98312 | tf_op jit(solution)/shard_map/ppermute | solution.py:13
  18.3 1.0 reshape.150
  19.4 0.7 pad_add_fusion
  20.1 0.7 pad_add_fusion.1
  20.7 1.0 compare_and_fusion
  22.2 0.4 fusion.39
  22.6 0.2 fusion.20
  22.9 0.3 fusion.19
  23.2 0.2 copy.38
  23.5 10.6 %all_to_all.29 = bf16[8,64,128]{2,1,0:T(8,128)(2,1)S(1)} all-to-all(bf16[8,64,128]{2,1,0:T(8,128)(2,1)S(1)} %reshape.151), channel_id=1, replica_groups=mesh['sp'=64,'tp'=8] {'tp'}, dimensions={0} | all-to-all | bytes 262144 | tf_op jit(solution)/shard_map/all_to_all | solution.py:122
  34.1 3.2 %multiply_reduce_fusion = (f32[64]{0:T(128)S(1)}, f32[64,2048]{1,0:T(8,128)S(1)}) fusion(bf16[1024,2048]{1,0:T(8,128)(2,1)} %param.17, bf16[64,2048]{1,0:T(8,128)(2,1)S(1)} %copy-done, bf16[8,64,128]{2,1,0:T(8,128)(2,1)S(1)} %all_to_all.29), kind=kOutput, calls=%fused_computation.23 | convolution fusion | flops 268959680 | bytes 5112064 | tf_op jit(solution)/shard_map/dot_general | solution.py:123
  37.5 0.2 broadcast_in_dim.16
  37.7 29.5 %all_to_all.30 = bf16[8,64,2048]{2,1,0:T(8,128)(2,1)S(1)} all-to-all(bf16[8,64,2048]{2,1,0:T(8,128)(2,1)S(1)} %broadcast_in_dim.16), channel_id=1, replica_groups=mesh['sp'=64,'tp'=8] {'tp'}, dimensions={0} | all-to-all | bytes 4194304 | tf_op jit(solution)/shard_map/all_to_all | solution.py:38
  67.2 50.1 %all-gather.2.cloned.1.call-done = bf16[2048,2112]{1,0:T(8,128)(2,1)} async-done(((bf16[32,2112]{1,0:T(8,128)(2,1)}), bf16[2048,2112]{1,0:T(8,128)(2,1)}) %all-gather.2.cloned.1.call-update) | async-done | bytes 8650768 | tf_op jit(solution)/shard_map/all_gather | solution.py:20
  117.3 4.7 %fusion.4 = f32[512,704]{0,1:T(8,128)} fusion(bf16[512,2048]{1,0:T(8,128)(2,1)S(1)} %bitcast.48, bf16[2048,2112]{1,0:T(8,128)(2,1)} %all-gather.2.cloned.1.call-done), kind=kOutput, calls=%fused_computation.5 | convolution fusion | flops 1476395008 | bytes 6684672 | tf_op jit(solution)/shard_map/dot_general | solution.py:127
  121.9 9.5 %fusion.6 = bf16[512,2048]{1,0:T(8,128)(2,1)} fusion(bf16[2048,2112]{1,0:T(8,128)(2,1)} %all-gather.2.cloned.1.call-done, bf16[512,2048]{1,0:T(8,128)(2,1)S(1)} %bitcast.49, f32[512,704]{0,1:T(8,128)} %fusion.4), kind=kOutput, calls=%fused_computation.7 | convolution fusion | flops 2956001280 | bytes 11927552 | tf_op jit(solution)/shard_map/dot_general | solution.py:131
  131.4 31.3 %all_to_all.31 = bf16[8,64,2048]{2,1,0:T(8,128)(2,1)S(1)} all-to-all(bf16[8,64,2048]{2,1,0:T(8,128)(2,1)} %bitcast.50), channel_id=1, replica_groups=mesh['sp'=64,'tp'=8] {'tp'}, dimensions={0} | all-to-all | bytes 4194304 | tf_op jit(solution)/shard_map/all_to_all | solution.py:52
  162.7 0.4 convert_reduce_fusion
  163.1 0.8 add_convert_fusion
  (26 shorter events, 1.1 us)
Async XLA Ops:
  6.5 110.7 %all-gather.2.cloned.1.call-start = ((), (), s32[]{:S(2)}) async-start(), calls=%async_computation.3 | async-start | bytes 9052160 | tf_op jit(solution)/shard_map/all_gather | solution.py:20
  8.2 14.4 %copy-start.2 = (f32[2]{0:T(128)S(1)}, f32[2]{0:T(128)}, u32[]{:S(2)}) copy-start(f32[2]{0:T(128)} %param.16) | copy-start | bytes 28
  8.9 10.5 %collective-permute-start.1 = (bf16[128]{0:T(256)(128)(2,1)S(1)}, bf16[128]{0:T(256)(128)(2,1)S(1)}, u32[]{:S(2)}, u32[]{:S(2)}) collective-permute-start(bf16[128]{0:T(256)(128)(2,1)S(1)} %slice.48), channel_id=1, source_target_pairs={{0,8},{8,16},{16,24},{24,32},{32,40},{40,48},{48,56},{56,64},{64,7... | collective-permute-start | bytes 776 | tf_op jit(solution)/shard_map/ppermute | solution.py:13
  14.9 6.8 %collective-permute-start = (bf16[128,128]{1,0:T(8,128)(2,1)S(1)}, bf16[128,128]{1,0:T(8,128)(2,1)S(1)}, u32[]{:S(2)}, u32[]{:S(2)}) collective-permute-start(bf16[128,128]{1,0:T(8,128)(2,1)S(1)} %fusion.35), channel_id=1, source_target_pairs={{0,8},{8,16},{16,24},{24,32},{32,40},{40,48},{48,56},{56,64},{64,7... | collective-permute-start | bytes 98312 | tf_op jit(solution)/shard_map/ppermute | solution.py:13
  22.9 11.2 %copy-start = (bf16[64,2048]{1,0:T(8,128)(2,1)S(1)}, bf16[64,2048]{1,0:T(8,128)(2,1)}, u32[]{:S(2)}) copy-start(bf16[64,2048]{1,0:T(8,128)(2,1)} %param.11) | copy-start | bytes 786436
  34.1 3.2 %copy-start.1 = (f32[2048]{0:T(1024)S(1)}, f32[2048]{0:T(1024)}, u32[]{:S(2)}) copy-start(f32[2048]{0:T(1024)} %param.18) | copy-start | bytes 24580
Sparse Core Ops, SparseCore 0:
  10.3 106.8 all-gather.1
where the time goes:
time: 171 us
  blocking collectives  71.3 us (42%)
  waiting for transfers between devices  50.1 us (29%)
  matrix products  18 us (11%)
  between operations  13.6 us (8%)
  starting transfers between devices  7.21 us (4%)
  local copies, waits for them, and re-layouts  5.42 us (3%)
  other arithmetic  5 us (3%)
    all_gather x1, waiting for transfers between devices, rows_first(): whole = lax.all_gather(both, axis, axis=0, tiled=True)  50.1 us
    all_to_all x1, blocking collectives, sum_at_owner(): tiles = lax.all_to_all(in_blocks(x, dim, size), axis, 0, 0, tiled=True)  31.3 us
    all_to_all x1, blocking collectives, from_everyone(): lax.all_to_all(jnp.broadcast_to(x[None], (size, *x.shape)), axis, 0, 0, t...  29.5 us
    all_to_all x1, blocking collectives, shards(): lax.all_to_all(attended, 'tp', split_axis=0, concat_axis=1, tiled=True)  10.6 us
    dot_general x1, matrix products, shards(): jnp.dot(hidden, down_whole, preferred_element_type=jnp.float32)  9.48 us
    ppermute x2, starting transfers between devices, passed_along(): lax.ppermute(value, axis, [(source, source + steps) for source in range(f...  7.21 us
    dot_general x1, matrix products, shards(): gate_acts = jnp.dot(normed, gate_whole, preferred_element_type=jnp.float32)  4.67 us
  transfers between devices with their start and end apart: 3, of which 1 were waited for; matrix products, arithmetic and copies ran while one was open for 7% of the time, Pallas kernels for 0%

commit v1 on v0

--- a/solution.py
+++ b/solution.py
@@ -17,7 +17,9 @@
     turned = [jnp.moveaxis(a, dim, 0) for a, dim in zip(arrays, dims)]
     widths = [t[0].size for t in turned]
     both = jnp.concatenate([t.reshape(-1, w) for t, w in zip(turned, widths)], axis=1)
-    whole = lax.all_gather(both, axis, axis=0, tiled=True)
+    whole = jnp.concatenate(
+        lax.all_to_all(jnp.stack([both] * lax.axis_size(axis)), axis, 0, 0), axis=0
+    )
     tiles = jnp.split(whole, [sum(widths[:k]) for k in range(1, len(widths))], axis=1)
     return tuple(
         (

time: 171 us -> 342 us (2.00)
  the two profiles are of different devices: /device:TPU:1 before, /device:TPU:24 now
where the time goes in v1:
time: 342 us
  blocking collectives  271 us (79%)
  waiting for transfers between devices  28.6 us (8%)
  matrix products  16.2 us (5%)
  starting transfers between devices  11 us (3%)
  local copies, waits for them, and re-layouts  9.33 us (3%)
  other arithmetic  4.98 us (1%)
    all_to_all x1, blocking collectives, rows_first(): lax.all_to_all(jnp.stack([both] * lax.axis_size(axis)), axis, 0, 0)  231 us
    all_to_all x1, blocking collectives, sum_at_owner(): tiles = lax.all_to_all(in_blocks(x, dim, size), axis, 0, 0, tiled=True)  30.7 us
    all_to_all x1, waiting for transfers between devices, from_everyone(): lax.all_to_all(jnp.broadcast_to(x[None], (size, *x.shape)), axis, 0, 0, t...  27 us
    all_to_all x1, blocking collectives, shards(): lax.all_to_all(attended, 'tp', split_axis=0, concat_axis=1, tiled=True)  10.2 us
    dot_general x1, matrix products, shards(): jnp.dot(hidden, down_whole, preferred_element_type=jnp.float32)  9.5 us
    ppermute x2, starting transfers between devices, passed_along(): lax.ppermute(value, axis, [(source, source + steps) for source in range(f...  7.27 us
  transfers between devices with their start and end apart: 3, of which 2 were waited for; matrix products, arithmetic and copies ran while one was open for 1% of the time, Pallas kernels for 0%

profile of v1, /device:TPU:24, one launch (start us, length us, event | category | flops | bytes accessed | tf_op | source)
XLA Modules:
  0.0 341.8 jit_solution(11323738596201779134)
XLA Ops:
  0.0 1.0 copy.23
  1.0 1.0 copy.24
  2.0 4.7 %collective-permute-start = (bf16[128,128]{1,0:T(8,128)(2,1)S(1)}, bf16[128,128]{1,0:T(8,128)(2,1)S(1)}, u32[]{:S(2)}, u32[]{:S(2)}) collective-permute-start(bf16[128,128]{1,0:T(8,128)(2,1)S(1)} %fusion.35), channel_id=1, source_target_pairs={{0,8},{8,16},{16,24},{24,32},{32,40},{40,48},{48,56},{56,64},{64,7... | collective-permute-start | bytes 98312 | tf_op jit(solution)/shard_map/ppermute | solution.py:13
  6.7 0.7 convert.3
  7.4 2.6 collective-permute-start.1
  10.2 1.0 reshape.156
  11.2 1.7 collective-permute-done.1
  12.9 0.7 pad_add_fusion
  13.6 0.7 pad_add_fusion.1
  14.3 1.0 compare_and_fusion
  15.7 0.4 fusion.39
  17.1 10.2 %all_to_all.34 = bf16[8,64,128]{2,1,0:T(8,128)(2,1)S(1)} all-to-all(bf16[8,64,128]{2,1,0:T(8,128)(2,1)S(1)} %reshape.157), channel_id=1, replica_groups=mesh['sp'=64,'tp'=8] {'tp'}, dimensions={0} | all-to-all | bytes 262144 | tf_op jit(solution)/shard_map/all_to_all | solution.py:124
  27.3 3.2 multiply_reduce_fusion
  30.6 1.6 broadcast_in_dim.16
  32.2 3.7 %all-to-all-start.1 = ((bf16[8,64,2048]{2,1,0:T(8,128)(2,1)}), bf16[8,64,2048]{2,1,0:T(8,128)(2,1)S(1)}, u32[]{:S(2)}, u32[]{:S(2)}) async-start(bf16[8,64,2048]{2,1,0:T(8,128)(2,1)} %broadcast_in_dim.16), calls=%async_computation.1 | async-start | bytes 4194304 | tf_op jit(solution)/shard_map/all_to_all | solution.py:40
  36.1 27.0 %all-to-all-done.1 = bf16[8,64,2048]{2,1,0:T(8,128)(2,1)S(1)} async-done(((bf16[8,64,2048]{2,1,0:T(8,128)(2,1)}), bf16[8,64,2048]{2,1,0:T(8,128)(2,1)S(1)}, u32[]{:S(2)}, u32[]{:S(2)}) %all-to-all-start.1) | async-done | bytes 2097184 | tf_op jit(solution)/shard_map/all_to_all | solution.py:40
  63.1 0.6 stack.2
  63.7 230.5 %all_to_all.35 = bf16[64,32,2112]{2,1,0:T(8,128)(2,1)S(1)} all-to-all(bf16[64,32,2112]{2,1,0:T(8,128)(2,1)S(1)} %stack.2), channel_id=1, replica_groups=mesh['sp'=64,'tp'=8] {'sp'}, dimensions={0} | all-to-all | bytes 17301504 | tf_op jit(solution)/shard_map/all_to_all | solution.py:21
  294.2 3.4 %copy-done = bf16[64,32,2112]{2,1,0:T(8,128)(2,1)} copy-done((bf16[64,32,2112]{2,1,0:T(8,128)(2,1)}, bf16[64,32,2112]{2,1,0:T(8,128)(2,1)S(1)}, u32[]{:S(2)}) %copy-start) | copy-done | bytes 8650776
  297.6 2.8 fusion.4
  300.4 9.5 %fusion.6 = bf16[512,2048]{1,0:T(8,128)(2,1)} fusion(bf16[2048,2112]{1,0:T(8,128)(2,1)} %bitcast.50, bf16[512,2048]{1,0:T(8,128)(2,1)S(1)} %bitcast.52, f32[512,704]{0,1:T(8,128)} %fusion.4), kind=kOutput, calls=%fused_computation.7 | convolution fusion | flops 2956001280 | bytes 11927552 | tf_op jit(solution)/shard_map/dot_general | solution.py:133
  309.9 30.7 %all_to_all.36 = bf16[8,64,2048]{2,1,0:T(8,128)(2,1)S(1)} all-to-all(bf16[8,64,2048]{2,1,0:T(8,128)(2,1)} %bitcast.53), channel_id=1, replica_groups=mesh['sp'=64,'tp'=8] {'tp'}, dimensions={0} | all-to-all | bytes 4194304 | tf_op jit(solution)/shard_map/all_to_all | solution.py:54
  340.6 0.3 convert_reduce_fusion
  341.0 0.8 add_convert_fusion
  (34 shorter events, 1.8 us)
Async XLA Ops:
  0.0 16.1 %copy-start.6 = (f32[2]{0:T(128)S(1)}, f32[2]{0:T(128)}, u32[]{:S(2)}) copy-start(f32[2]{0:T(128)} %param.16) | copy-start | bytes 28
  2.0 13.3 %collective-permute-start = (bf16[128,128]{1,0:T(8,128)(2,1)S(1)}, bf16[128,128]{1,0:T(8,128)(2,1)S(1)}, u32[]{:S(2)}, u32[]{:S(2)}) collective-permute-start(bf16[128,128]{1,0:T(8,128)(2,1)S(1)} %fusion.35), channel_id=1, source_target_pairs={{0,8},{8,16},{16,24},{24,32},{32,40},{40,48},{48,56},{56,64},{64,7... | collective-permute-start | bytes 98312 | tf_op jit(solution)/shard_map/ppermute | solution.py:13
  7.4 5.5 %collective-permute-start.1 = (bf16[128]{0:T(256)(128)(2,1)S(1)}, bf16[128]{0:T(256)(128)(2,1)S(1)}, u32[]{:S(2)}, u32[]{:S(2)}) collective-permute-start(bf16[128]{0:T(256)(128)(2,1)S(1)} %slice.48), channel_id=1, source_target_pairs={{0,8},{8,16},{16,24},{24,32},{32,40},{40,48},{48,56},{56,64},{64,7... | collective-permute-start | bytes 776 | tf_op jit(solution)/shard_map/ppermute | solution.py:13
  16.4 10.9 %copy-start.1 = (bf16[64,2048]{1,0:T(8,128)(2,1)S(1)}, bf16[64,2048]{1,0:T(8,128)(2,1)}, u32[]{:S(2)}) copy-start(bf16[64,2048]{1,0:T(8,128)(2,1)} %param.11) | copy-start | bytes 786436
  27.3 3.2 copy-start.5
  32.2 3.8 %copy-start.2 = (bf16[32,704]{1,0:T(8,128)(2,1)S(1)}, bf16[32,704]{1,0:T(8,128)(2,1)}, u32[]{:S(2)}) copy-start(bf16[32,704]{1,0:T(8,128)(2,1)} %param.19) | copy-start | bytes 135172
  32.2 3.8 %copy-start.3 = (bf16[32,704]{1,0:T(8,128)(2,1)S(1)}, bf16[32,704]{1,0:T(8,128)(2,1)}, u32[]{:S(2)}) copy-start(bf16[32,704]{1,0:T(8,128)(2,1)} %param.20) | copy-start | bytes 135172
  32.2 3.8 %copy-start.4 = (bf16[704,32]{0,1:T(8,128)(2,1)S(1)}, bf16[704,32]{0,1:T(8,128)(2,1)}, u32[]{:S(2)}) copy-start(bf16[704,32]{0,1:T(8,128)(2,1)} %param.21) | copy-start | bytes 135172
  32.2 30.8 %all-to-all-start.1 = ((bf16[8,64,2048]{2,1,0:T(8,128)(2,1)}), bf16[8,64,2048]{2,1,0:T(8,128)(2,1)S(1)}, u32[]{:S(2)}, u32[]{:S(2)}) async-start(bf16[8,64,2048]{2,1,0:T(8,128)(2,1)} %broadcast_in_dim.16), calls=%async_computation.1 | async-start | bytes 4194304 | tf_op jit(solution)/shard_map/all_to_all | solution.py:40
  294.2 3.4 %copy-start = (bf16[64,32,2112]{2,1,0:T(8,128)(2,1)}, bf16[64,32,2112]{2,1,0:T(8,128)(2,1)S(1)}, u32[]{:S(2)}) copy-start(bf16[64,32,2112]{2,1,0:T(8,128)(2,1)S(1)} %all_to_all.35) | copy-start | bytes 25952260
